TPU v7x, 32 devices: a whole 2x2x4 slice. The times are simulated.
32 devices in a mesh: sp: 8 (over z, x), tp: 4 (over y, core).
Axes of the slice: x: 2, y: 2, z: 4, core: 2. Of those that a mesh axis runs over, the one named last changes fastest.
Arguments:
- inputs: bfloat16 [2048, 2048], P('sp', 'tp'), may hold values from -120 to 120
- in_gain: float32 [2048], replicated, may hold values from 0.1 to 1.9
- query_weight: bfloat16 [2048, 1024], P('sp', 'tp'), may hold values from -0.125 to 0.125
- key_weight: bfloat16 [2048, 1024], P('sp', 'tp'), may hold values from -0.125 to 0.125
- value_weight: bfloat16 [2048, 1024], P('sp', 'tp'), may hold values from -0.125 to 0.125
- beta_weight: bfloat16 [2, 2048, 8], replicated, may hold values from -0.125 to 0.125
- decay_weight: bfloat16 [2, 2048, 8], replicated, may hold values from -0.125 to 0.125
- beta_shift: float32 [2, 8], replicated, may hold values from -9 to 1
- decay_pace: float32 [2, 8, 2048], P(None, 'tp', 'sp'), may hold values from 0 to 0.1
- decay_jolt: float32 [2, 8, 2048], P(None, 'tp', 'sp'), may hold values from -1.4 to 0, as said below
- head_gain: float32 [128], replicated, may hold values from 0.1 to 1.9
- glu_value_weight: bfloat16 [2048, 1024], P('sp', 'tp'), may hold values from -0.125 to 0.125
- glu_gate_weight: bfloat16 [2048, 1024], P('sp', 'tp'), may hold values from -0.125 to 0.125
- conv_kernel: bfloat16 [31, 1024], P(None, 'tp'), may hold values from -4 to 4
- conv_gain: float32 [1024], P('tp'), may hold values from 0.1 to 1.9
- out_delta_weight: bfloat16 [1024, 2048], P('tp', 'sp'), may hold values from -0.125 to 0.125
- out_conv_weight: bfloat16 [1024, 2048], P('tp', 'sp'), may hold values from -0.125 to 0.125
Outputs:
- mixed: bfloat16 [2048, 2048], P(('sp', 'tp'))
Inputs may be any that keep to these rules, and one draw needn't show every extreme that they name: `decay_jolt`: zero but at a few positions of each direction and head.
All inputs are finite; a program needn't handle non-finite values.
Results may differ from a plain program's by a relative error of at most 0.017.
Values may be sent and summed in bfloat16 or wider, within the bound.
A program may use at most 128 MiB of HBM per device.

v0:
```python
import functools

import jax
import jax.numpy as jnp
from jax import lax
from jax.experimental import pallas as pl
from jax.experimental.pallas import tpu as pltpu
from jax.sharding import PartitionSpec as P

HEAD = 128
QK_HEADS = 8
V_HEADS = 8
CONV_CH = 1024
KERNEL = 31
BLOCK = 64


highest = lax.Precision.HIGHEST


def prefix_2(shard, axis, combine, identity, reverse):
    peers, position = (lax.axis_size(axis), lax.axis_index(axis))
    everything = jax.tree.map(
        lambda part, kind: lax.all_gather(part.astype(kind), axis),
        shard,
        (jnp.bfloat16, jnp.bfloat16),
    )
    start = jax.tree.map(
        lambda part, zero: jnp.broadcast_to(jnp.asarray(zero, part.dtype), part.shape),
        shard,
        identity,
    )

    def lap(k, before):
        at = peers - 1 - k if reverse else k
        reached = at > position if reverse else at < position
        new = combine(
            before, jax.tree.map(lambda part, own: part[at].astype(own.dtype), everything, shard)
        )
        return jax.tree.map(lambda a, b: jnp.where(reached, a, b), new, before)

    return lax.fori_loop(0, peers, lap, start)


def padded_2(cells, sides, width):
    for axis, dim in sides:
        count = lax.axis_size(axis)
        ends = count - 1
        head = lax.slice_in_dim(cells, 0, width, axis=dim)
        tail = lax.slice_in_dim(cells, cells.shape[dim] - width, cells.shape[dim], axis=dim)
        cells = jnp.concatenate(
            [
                lax.ppermute(tail, axis, [(i, (i + 1) % count) for i in range(ends)]),
                cells,
                lax.ppermute(head, axis, [((i + 1) % count, i) for i in range(ends)]),
            ],
            axis=dim,
        )
    return cells


def matmul_high(left_side, right_side):
    return jnp.matmul(left_side, right_side, precision=highest)


def unit_lower_inverse(matrix):
    order_size = matrix.shape[-1]
    leading = matrix.shape[:-2]
    inverse = jnp.ones(leading + (order_size, 1, 1), jnp.float32)
    size_now = 1
    while size_now < order_size:
        pair_count = order_size // (2 * size_now)
        halves = inverse.reshape(leading + (pair_count, 2, size_now, size_now))
        upper_inv = halves[..., 0, :, :]
        lower_inv = halves[..., 1, :, :]
        block_grid = matrix.reshape(leading + (pair_count, 2 * size_now, pair_count, 2 * size_now))
        diagonal = jnp.moveaxis(jnp.diagonal(block_grid, axis1=-4, axis2=-2), -1, -3)
        corner = diagonal[..., size_now:, :size_now]
        below = -matmul_high(lower_inv, matmul_high(corner, upper_inv))
        top_half = jnp.concatenate([upper_inv, jnp.zeros_like(below)], axis=-1)
        bottom_half = jnp.concatenate([below, lower_inv], axis=-1)
        inverse = jnp.concatenate([top_half, bottom_half], axis=-2)
        size_now = 2 * size_now
    return inverse.reshape(leading + (order_size, order_size))


def block_terms(queries, key_rows, values, beta_gate, log_decay):
    span = key_rows.shape[-2]
    cumulative = jnp.cumsum(log_decay, axis=-1)
    lower_mask = jnp.tril(jnp.ones((span, span), dtype=bool))
    strict = jnp.tril(jnp.ones((span, span), dtype=bool), -1)
    log_gap = cumulative[..., :, None] - cumulative[..., None, :]
    decay_mask = jnp.where(lower_mask, jnp.exp(jnp.where(lower_mask, log_gap, 0.0)), 0.0)
    key_inner = matmul_high(key_rows, jnp.swapaxes(key_rows, -1, -2))
    below_part = jnp.where(strict, beta_gate[..., :, None] * key_inner * decay_mask, 0.0)
    inverse = unit_lower_inverse(below_part + jnp.eye(span, dtype=jnp.float32))
    fresh = matmul_high(inverse, values * beta_gate[..., None])
    weighted = matmul_high(inverse, key_rows * (beta_gate * jnp.exp(cumulative))[..., None])
    scores = matmul_high(queries, jnp.swapaxes(key_rows, -1, -2)) * decay_mask
    readout = queries * jnp.exp(cumulative)[..., None] - matmul_high(scores, weighted)
    tail_keys = jnp.swapaxes(
        key_rows * jnp.exp(cumulative[..., -1:] - cumulative)[..., None], -1, -2
    )
    identity = jnp.eye(key_rows.shape[-1], dtype=jnp.float32)
    carry_map = jnp.exp(cumulative[..., -1])[..., None, None] * identity - matmul_high(
        tail_keys, weighted
    )
    carry_add = matmul_high(tail_keys, fresh)
    within = matmul_high(scores, fresh)
    return (carry_map, carry_add, readout, within)


def layer_norm_rows(inputs, gain):
    as_float = inputs.astype(jnp.float32)
    mean_row = jnp.mean(as_float, axis=-1, keepdims=True)
    spread = jnp.mean(jnp.square(as_float - mean_row), axis=-1, keepdims=True)
    return ((as_float - mean_row) * lax.rsqrt(spread + 1e-05) * gain).astype(jnp.bfloat16)


def compose(earlier, later):
    return (matmul_high(later[0], earlier[0]), matmul_high(later[0], earlier[1]) + later[1])


def local_maps(queries, key_rows, values, beta_gate, log_decay):
    head_count, length_dev, key_width = queries.shape
    value_width = values.shape[-1]
    block_count = length_dev // BLOCK

    def split_blocks(tensor):
        return tensor.reshape((head_count, block_count, BLOCK) + tensor.shape[2:])

    carry_map, carry_add, readout, within = block_terms(
        split_blocks(queries),
        split_blocks(key_rows),
        split_blocks(values),
        split_blocks(beta_gate),
        split_blocks(log_decay),
    )
    identity = jnp.broadcast_to(
        jnp.eye(key_width, dtype=jnp.float32), (head_count, key_width, key_width)
    )
    nothing = jnp.zeros((head_count, key_width, value_width), jnp.float32)

    def advance(prefix, block_parts):
        prefix_map, prefix_add = prefix
        step_map, step_add, step_read = block_parts
        reach_now = matmul_high(step_read, prefix_map)
        offset_now = matmul_high(step_read, prefix_add)
        return (
            (matmul_high(step_map, prefix_map), matmul_high(step_map, prefix_add) + step_add),
            (reach_now, offset_now),
        )

    moved = (
        jnp.moveaxis(carry_map, 1, 0),
        jnp.moveaxis(carry_add, 1, 0),
        jnp.moveaxis(readout, 1, 0),
    )
    totals, (reach_map, offset) = lax.scan(advance, (identity, nothing), moved)
    reach_map = jnp.moveaxis(reach_map, 0, 1).reshape(head_count, length_dev, key_width)
    offset = (jnp.moveaxis(offset, 0, 1) + within).reshape(head_count, length_dev, value_width)
    return (totals, reach_map, offset)


def on_device(
    inputs,
    in_gain,
    query_weight,
    key_weight,
    value_weight,
    beta_weight,
    decay_weight,
    beta_shift,
    decay_pace,
    decay_jolt,
    head_gain,
    glu_value_weight,
    glu_gate_weight,
    conv_kernel,
    conv_gain,
    out_delta_weight,
    out_conv_weight,
):
    gathered = lax.all_gather(inputs, "tp", axis=1, tiled=True)
    normed = layer_norm_rows(gathered, in_gain)
    row_count = normed.shape[0]

    def add_rows(shard_rows):
        return jnp.dot(normed, shard_rows, preferred_element_type=jnp.float32)

    shards = (
        lax.all_gather(query_weight, "sp", axis=0, tiled=True),
        lax.all_gather(key_weight, "sp", axis=0, tiled=True),
        lax.all_gather(value_weight, "sp", axis=0, tiled=True),
        lax.all_gather(glu_value_weight, "sp", axis=0, tiled=True),
        lax.all_gather(glu_gate_weight, "sp", axis=0, tiled=True),
    )
    projected = tuple((add_rows(shard_rows) for shard_rows in shards))
    delta_sums = projected[:3]
    conv_sums = projected[3:]
    queries, key_proj, value_proj = (summed.astype(jnp.bfloat16) for summed in delta_sums)
    local_heads = value_proj.shape[1] // HEAD
    group_size = V_HEADS // QK_HEADS
    head_first = lax.axis_index("tp") * local_heads

    def by_head(matrix, head_total):
        return jnp.transpose(
            matrix.astype(jnp.float32).reshape(row_count, head_total, HEAD), (1, 0, 2)
        )

    query_heads = jnp.repeat(
        jax.nn.silu(by_head(queries, local_heads // group_size)), group_size, axis=0
    )
    key_heads = jax.nn.silu(by_head(key_proj, local_heads // group_size))
    key_heads = key_heads * lax.rsqrt(
        jnp.sum(jnp.square(key_heads), axis=-1, keepdims=True) + 1e-06
    )
    key_heads = jnp.repeat(key_heads, group_size, axis=0)
    value_heads = by_head(value_proj, local_heads)
    own_beta = lax.dynamic_slice_in_dim(beta_weight, head_first, local_heads, 2)
    own_decay = lax.dynamic_slice_in_dim(decay_weight, head_first, local_heads, 2)
    beta_pre = jnp.einsum("td,edh->eht", normed, own_beta, preferred_element_type=jnp.float32)
    decay_pre = jnp.einsum("td,edh->eht", normed, own_decay, preferred_element_type=jnp.float32)
    own_shift = lax.dynamic_slice_in_dim(beta_shift, head_first, local_heads, 1)
    beta_gate = jax.nn.sigmoid(beta_pre + own_shift[:, :, None])
    log_decay = -decay_pace * jax.nn.softplus(decay_pre) + decay_jolt
    identity = jnp.broadcast_to(jnp.eye(HEAD, dtype=jnp.float32), (local_heads, HEAD, HEAD))
    nothing = jnp.zeros((local_heads, HEAD, HEAD), jnp.float32)
    forward_maps, forward_reach, forward_offset = local_maps(
        query_heads, key_heads, value_heads, beta_gate[0], log_decay[0]
    )
    entry_forward = prefix_2(
        (forward_maps[0], forward_maps[1]), "sp", compose, (identity, nothing), False
    )
    forward_out = matmul_high(forward_reach, entry_forward[1]) + forward_offset
    backward_maps, backward_reach, backward_offset = local_maps(
        jnp.flip(query_heads, 1),
        jnp.flip(key_heads, 1),
        jnp.flip(value_heads, 1),
        jnp.flip(beta_gate[1], 1),
        jnp.flip(log_decay[1], 1),
    )
    entry_backward = prefix_2(
        (backward_maps[0], backward_maps[1]), "sp", compose, (identity, nothing), True
    )
    backward_out = jnp.flip(matmul_high(backward_reach, entry_backward[1]) + backward_offset, 1)
    combined = forward_out + backward_out
    scaled = (
        combined
        * lax.rsqrt(jnp.mean(jnp.square(combined), axis=-1, keepdims=True) + 1e-06)
        * head_gain
    )
    delta_out = (
        jnp.transpose(scaled, (1, 0, 2)).reshape(row_count, local_heads * HEAD).astype(jnp.bfloat16)
    )
    glu_value, glu_gate = (summed.astype(jnp.bfloat16) for summed in conv_sums)
    gated = (glu_value.astype(jnp.float32) * jax.nn.sigmoid(glu_gate.astype(jnp.float32))).astype(
        jnp.bfloat16
    )
    padded = padded_2(gated, (("sp", 0),), KERNEL // 2)
    filtered = jnp.zeros(gated.shape, jnp.float32)
    for tap_index in range(KERNEL):
        filtered = filtered + padded[tap_index : tap_index + row_count].astype(
            jnp.float32
        ) * conv_kernel[tap_index].astype(jnp.float32)
    totals = lax.psum((jnp.sum(filtered, axis=1), jnp.sum(filtered * filtered, axis=1)), "tp")
    mean_row = totals[0][:, None] / CONV_CH
    second = totals[1][:, None] / CONV_CH
    conv_out = jax.nn.silu(
        (filtered - mean_row) * lax.rsqrt(second - mean_row * mean_row + 1e-05) * conv_gain
    ).astype(jnp.bfloat16)
    delta_whole, conv_whole = (
        lax.all_gather(out_delta_weight, "sp", axis=1, tiled=True),
        lax.all_gather(out_conv_weight, "sp", axis=1, tiled=True),
    )
    delta_part = jnp.dot(delta_out, delta_whole, preferred_element_type=jnp.float32)
    conv_part = jnp.dot(conv_out, conv_whole, preferred_element_type=jnp.float32)
    return lax.psum_scatter(
        (delta_part + conv_part).astype(jnp.bfloat16), "tp", scatter_dimension=0, tiled=True
    )


MESH = pl.DeviceIdType.MESH
F32 = jnp.float32
BF16 = jnp.bfloat16
VM = pl.BlockSpec(memory_space=pltpu.VMEM)


def greet(peers):
    barrier = pltpu.get_barrier_semaphore()
    for peer in peers:
        pl.semaphore_signal(barrier, inc=1, device_id=peer, device_id_type=MESH)
    pl.semaphore_wait(barrier, len(peers))


def ring_peers(n):
    s, t = lax.axis_index("sp"), lax.axis_index("tp")
    half = n // 2
    z, x = s // 2, s % 2
    partner = (z * 2 + (1 - x), t)
    stride = [(((z + d) % half) * 2 + x, t) for d in range(1, half)]
    return s, t, z, x, half, partner, stride


def rcopy(src, dst, send, recv, peer):
    return pltpu.make_async_remote_copy(
        src_ref=src, dst_ref=dst, send_sem=send, recv_sem=recv, device_id=peer, device_id_type=MESH
    )


def dot(a, b):
    return jnp.dot(a, b, preferred_element_type=F32)


def project_kernel(n, nt, n_in, *refs):
    x_ref, gain_ref, wg_ref = refs[:3]
    w_refs = refs[3 : 3 + n_in]
    qkv_ref, gated_ref, pre_ref = refs[3 + n_in : 6 + n_in]
    xbuf, normed, acc, wz, wx, xs, xr, zs, zr, ps, pr = refs[6 + n_in :]
    s, t, z, x, half, partner, stride = ring_peers(n)
    others = [(s, (t + d) % nt) for d in range(1, nt)]
    greet(others + [partner] + stride)
    order = [d for d in range(half - 1)]
    x_copies = [rcopy(x_ref, xbuf.at[d], xs.at[d], xr.at[d], others[d]) for d in range(nt - 1)]
    for c in x_copies:
        c.start()
    own_x = [rcopy(w_refs[w], wx.at[0, w], ps.at[0, w], pr.at[0, w], partner) for w in range(n_in)]
    own_z = [
        [rcopy(w_refs[w], wz.at[d, w], zs.at[d, w], zr.at[d, w], stride[d]) for d in order]
        for w in range(n_in)
    ]
    for w in range(n_in):
        for d in order:
            own_z[w][d].start()
        own_x[w].start()
    for c in x_copies:
        c.wait_recv()
    rows, part = x_ref.shape
    block = w_refs[0].shape[0]
    per = part // block
    total = rows * 0 + part * nt
    chunks = [(t, x_ref)] + [((t + nt - 1 - d) % nt, xbuf.at[d]) for d in range(nt - 1)]
    mean = sum(jnp.sum(r[...].astype(F32), axis=1, keepdims=True) for _, r in chunks) / total
    var = (
        sum(jnp.sum(jnp.square(r[...].astype(F32) - mean), axis=1, keepdims=True) for _, r in chunks)
        / total
    )
    inv = lax.rsqrt(var + 1e-05)
    for src, r in chunks:
        y = (r[...].astype(F32) - mean) * inv
        for p in range(per):
            b = src * per + p
            g = gain_ref[pl.ds(b, 1), :]
            normed[b] = (y[:, p * block : (p + 1) * block] * g).astype(BF16)
    pre = dot(normed[0], wg_ref[0:block, :])
    for b in range(1, n):
        pre = pre + dot(normed[b], wg_ref[b * block : (b + 1) * block, :])
    pre_ref[...] = pre
    width = w_refs[0].shape[1]
    forwards = []
    for w in range(n_in):
        value = dot(normed[s], w_refs[w][...])
        for d in order:
            own_z[w][d].wait_recv()
            f = rcopy(wz.at[d, w], wx.at[d + 1, w], ps.at[d + 1, w], pr.at[d + 1, w], partner)
            f.start()
            forwards.append(f)
            src = ((z + half - 1 - d) % half) * 2 + x
            value = value + dot(normed[src], wz[d, w])
        acc[:, w * width : (w + 1) * width] = value
    for w in range(n_in):
        own_x[w].wait_recv()
        value = acc[:, w * width : (w + 1) * width]
        value = value + dot(normed[z * 2 + (1 - x)], wx[0, w])
        for d in order:
            forwards[w * len(order) + d].wait_recv()
            src = ((z + half - 1 - d) % half) * 2 + (1 - x)
            value = value + dot(normed[src], wx[d + 1, w])
        acc[:, w * width : (w + 1) * width] = value
    qkv_ref[...] = acc[:, : 3 * width].astype(BF16)
    glu_value = acc[:, 3 * width : 4 * width].astype(BF16).astype(F32)
    glu_gate = acc[:, 4 * width : 5 * width].astype(BF16).astype(F32)
    gated_ref[...] = (glu_value * jax.nn.sigmoid(glu_gate)).astype(BF16)
    for c in x_copies + own_x + forwards + [c for row in own_z for c in row]:
        c.wait_send()


def dot3(a, b):
    ah, bh = a.astype(BF16), b.astype(BF16)
    al, bl = (a - ah.astype(F32)).astype(BF16), (b - bh.astype(F32)).astype(BF16)
    return dot(ah, bh) + (dot(ah, bl) + dot(al, bh))


def delta_kernel(heads, qkv_ref, pre_ref, shift_ref, pace_ref, jolt_ref, ma_ref, read_ref, within_ref):
    span = qkv_ref.shape[0]
    width = heads * HEAD
    rows = jnp.transpose(pre_ref[...])
    beta = jax.nn.sigmoid(rows[0:8] + shift_ref[...])
    log_decay = -pace_ref[...] * jax.nn.softplus(rows[8:16]) + jolt_ref[...]
    i = lax.broadcasted_iota(jnp.int32, (span, span), 0)
    j = lax.broadcasted_iota(jnp.int32, (span, span), 1)
    high = lax.Precision.HIGHEST
    upto = jnp.dot(log_decay, (i <= j).astype(F32), precision=high, preferred_element_type=F32)
    onto = jnp.dot(log_decay, (i >= j).astype(F32), precision=high, preferred_element_type=F32)
    which = lax.broadcasted_iota(jnp.int32, (8, span), 0)
    cum = jnp.where(which < heads, upto, onto)
    cols = jnp.transpose(
        jnp.concatenate([beta, cum, jnp.zeros((128 - 16, span), F32)], axis=0)
    )
    eye = (i == j).astype(F32)
    eye_head = (
        lax.broadcasted_iota(jnp.int32, (HEAD, HEAD), 0)
        == lax.broadcasted_iota(jnp.int32, (HEAD, HEAD), 1)
    ).astype(F32)
    level = i ^ j
    for h in range(heads):
        lo = h * HEAD
        q = jax.nn.silu(qkv_ref[:, lo : lo + HEAD].astype(F32))
        k = jax.nn.silu(qkv_ref[:, width + lo : width + lo + HEAD].astype(F32))
        k = k * lax.rsqrt(jnp.sum(jnp.square(k), axis=1, keepdims=True) + 1e-06)
        v = qkv_ref[:, 2 * width + lo : 2 * width + lo + HEAD].astype(F32)
        kt = jnp.transpose(k)
        kk = dot3(k, kt)
        qk = dot(q.astype(BF16), kt.astype(BF16))
        total = jnp.zeros((span, HEAD), F32)
        for e in range(2):
            c = e * heads + h
            beta_col = cols[:, c : c + 1]
            cum_col = cols[:, 8 + c : 9 + c]
            cum_row = cum[c : c + 1, :]
            keep = (i >= j) if e == 0 else (i <= j)
            gap = jnp.exp(jnp.where(keep, cum_col - cum_row, 0.0))
            decay = jnp.where(keep, gap, 0.0)
            below = jnp.where(i == j, 0.0, beta_col * kk * decay)
            inverse = eye - jnp.where(level < 2, below, 0.0)
            size = 2
            while size < span:
                corner = jnp.where((level >= size) & (level < 2 * size), below, 0.0)
                inverse = inverse - dot3(inverse, dot3(corner, inverse))
                size = 2 * size
            grown = jnp.exp(cum_col)
            rhs = jnp.concatenate([v * beta_col, k * (beta_col * grown)], axis=1)
            solved = dot3(inverse, rhs)
            solved_b = solved.astype(BF16)
            out = dot((qk * decay).astype(BF16), solved_b)
            total = total + out[:, :HEAD]
            read_ref[c] = (q * grown - out[:, HEAD:]).astype(BF16)
            end = cum[c : c + 1, span - 1 : span] if e == 0 else cum[c : c + 1, 0:1]
            tail = jnp.transpose(k * jnp.exp(end - cum_col))
            state = dot3(tail, solved)
            ma_ref[c, :, :HEAD] = (jnp.exp(end) * eye_head - state[:, HEAD:]).astype(BF16)
            ma_ref[c, :, HEAD:] = state[:, :HEAD].astype(BF16)
        within_ref[h] = total


def finish_kernel(
    n, nt, heads, channels,
    ma_ref, read_ref, within_ref, gated_ref, taps_ref, cgain_ref, hgain_ref, ow_ref,
    out_ref,
    near, pair, far, halo, conv_pad, stat, stats, wz, wx, part, parts,
    ns, nr, fs, fr, hs, hr, ss, sr, zs, zr, ps, pr, rs, rr,
):
    s, t, z, x, half, partner, stride = ring_peers(n)
    others = [(s, (t + d) % nt) for d in range(1, nt)]
    greet(others + [((s + d) % n, t) for d in range(1, n)])
    rows, width = gated_ref.shape
    edge = 16

    def at(offset):
        return ((s + offset + n) % n, t)

    def inside(offset):
        return (s < n - offset) if offset > 0 else (s >= -offset)

    steps = []
    for d in (1, 2):
        for e in range(2):
            go = d if e == 0 else -d
            lo = e * heads
            steps.append((go, rcopy(ma_ref.at[pl.ds(lo, heads)], near.at[e, d - 1], ns.at[e, d - 1], nr.at[e, d - 1], at(go)), near.at[e, d - 1]))
    sides = [
        (1, rcopy(gated_ref.at[pl.ds(rows - edge, edge)], halo.at[0], hs.at[0], hr.at[0], at(1)), halo.at[0]),
        (-1, rcopy(gated_ref.at[pl.ds(0, edge)], halo.at[1], hs.at[1], hr.at[1], at(-1)), halo.at[1]),
    ]

    def start(moves):
        for go, copy, _ in moves:
            @pl.when(inside(go))
            def _():
                copy.start()

    def arrive(moves):
        for go, copy, slot in moves:
            @pl.when(inside(-go))
            def _():
                copy.wait_recv()

            @pl.when(jnp.logical_not(inside(-go)))
            def _():
                slot[...] = jnp.zeros(slot.shape, slot.dtype)

    def left(moves):
        for go, copy, _ in moves:
            @pl.when(inside(go))
            def _():
                copy.wait_send()

    start(steps)
    start(sides)
    own_z = [rcopy(ow_ref, wz.at[d], zs.at[d], zr.at[d], stride[d]) for d in range(half - 1)]
    own_x = rcopy(ow_ref, wx.at[0], ps.at[0], pr.at[0], partner)
    own_x.start()
    for c in own_z:
        c.start()
    arrive(steps)
    for e in range(2):
        for h in range(heads):
            first = near[e, 0, h]
            mixed = dot(first[:, :HEAD], near[e, 1, h])
            pair[e, h, :, :HEAD] = mixed[:, :HEAD].astype(BF16)
            pair[e, h, :, HEAD:] = (mixed[:, HEAD:] + first[:, HEAD:].astype(F32)).astype(BF16)
    hops = []
    for d in range(1, half):
        for e in range(2):
            go = 2 * d if e == 0 else -2 * d
            hops.append((go, rcopy(pair.at[e], far.at[e, d - 1], fs.at[e, d - 1], fr.at[e, d - 1], at(go)), far.at[e, d - 1]))
    start(hops)

    arrive(sides)
    conv_pad[0:edge, :] = halo[0].astype(F32)
    conv_pad[edge : edge + rows, :] = gated_ref[...].astype(F32)
    conv_pad[edge + rows : 2 * edge + rows, :] = halo[1].astype(F32)
    taps = taps_ref[...].astype(F32)
    count = taps.shape[0]
    base = edge - count // 2
    filtered = conv_pad[base : base + rows, :] * taps[0:1, :]
    for tap in range(1, count):
        filtered = filtered + conv_pad[base + tap : base + tap + rows, :] * taps[tap : tap + 1, :]
    sum_col = jnp.sum(filtered, axis=1, keepdims=True)
    square_col = jnp.sum(filtered * filtered, axis=1, keepdims=True)
    lane = lax.broadcasted_iota(jnp.int32, (rows, 128), 1)
    stat[...] = jnp.transpose(jnp.where(lane == 0, sum_col, jnp.where(lane == 1, square_col, 0.0)))[0:8]
    stat_copies = [rcopy(stat, stats.at[d], ss.at[d], sr.at[d], others[d]) for d in range(nt - 1)]
    for c in stat_copies:
        c.start()

    forwards = []
    for d in range(half - 1):
        own_z[d].wait_recv()
        f = rcopy(wz.at[d], wx.at[d + 1], ps.at[d + 1], pr.at[d + 1], partner)
        f.start()
        forwards.append(f)

    for c in stat_copies:
        c.wait_recv()
    whole = stat[...]
    for d in range(nt - 1):
        whole = whole + stats[d]
    back = jnp.transpose(jnp.concatenate([whole, jnp.zeros((120, rows), F32)], axis=0))
    mean = back[:, 0:1] / channels
    second = back[:, 1:2] / channels
    conv_out = jax.nn.silu(
        (filtered - mean) * lax.rsqrt(second - mean * mean + 1e-05) * cgain_ref[...]
    ).astype(BF16)

    arrive(hops)
    delta_heads = []
    for h in range(heads):
        o = within_ref[h]
        for e in range(2):
            entry = jnp.zeros((HEAD, HEAD), F32)
            for d in range(half - 2, -1, -1):
                m = far[e, d, h]
                entry = dot(m[:, :HEAD], entry.astype(BF16)) + m[:, HEAD:].astype(F32)
            m = pair[e, h]
            entry = dot(m[:, :HEAD], entry.astype(BF16)) + m[:, HEAD:].astype(F32)
            o = o + dot(read_ref[e * heads + h], entry.astype(BF16))
        o = o * lax.rsqrt(jnp.mean(jnp.square(o), axis=1, keepdims=True) + 1e-06) * hgain_ref[...]
        delta_heads.append(o.astype(BF16))
    both = jnp.concatenate(delta_heads + [conv_out], axis=1)
    block = ow_ref.shape[1]
    piece = rows // nt

    def emit(src, weights):
        value = dot(both, weights).astype(BF16)
        column = pl.ds(pl.multiple_of(src * block, block), block)
        for p in range(nt):
            part[p, :, column] = value[p * piece : (p + 1) * piece]

    emit(s, ow_ref[...])
    for d in range(half - 1):
        emit(((z + half - 1 - d) % half) * 2 + x, wz[d])
    own_x.wait_recv()
    emit(z * 2 + (1 - x), wx[0])
    for d in range(half - 1):
        forwards[d].wait_recv()
        emit(((z + half - 1 - d) % half) * 2 + (1 - x), wx[d + 1])
    sums = [rcopy(part.at[(t + d) % nt], parts.at[d - 1], rs.at[d - 1], rr.at[d - 1], others[d - 1]) for d in range(1, nt)]
    for c in sums:
        c.start()
    for c in sums:
        c.wait_recv()
    mixed = part[t].astype(F32)
    for d in range(nt - 1):
        mixed = mixed + parts[d].astype(F32)
    out_ref[...] = mixed.astype(BF16)
    left(steps)
    left(sides)
    left(hops)
    for c in own_z + [own_x] + forwards + stat_copies + sums:
        c.wait_send()


def fast_device(
    n, nt,
    inputs, in_gain, query_weight, key_weight, value_weight, beta_weight, decay_weight,
    beta_shift, decay_pace, decay_jolt, head_gain, glu_value_weight, glu_gate_weight,
    conv_kernel, conv_gain, out_delta_weight, out_conv_weight,
):
    rows, part = inputs.shape
    block, width = query_weight.shape
    heads = decay_pace.shape[1]
    half = n // 2
    depth = in_gain.shape[0]
    channels = conv_kernel.shape[1] * nt
    first = lax.axis_index("tp") * heads

    def gate_columns(weight):
        own = lax.dynamic_slice_in_dim(weight, first, heads, 2)
        own = jnp.moveaxis(own, 0, 1).reshape(depth, 2 * heads)
        return jnp.pad(own, ((0, 0), (0, 8 - 2 * heads)))

    gate_weight = jnp.pad(
        jnp.concatenate([gate_columns(beta_weight), gate_columns(decay_weight)], axis=1),
        ((0, 0), (0, 112)),
    )
    pad_rows = ((0, 8 - 2 * heads), (0, 0))
    shift = jnp.pad(
        lax.dynamic_slice_in_dim(beta_shift, first, heads, 1).reshape(2 * heads, 1), pad_rows
    )
    pace = jnp.pad(decay_pace.reshape(2 * heads, rows), pad_rows)
    jolt = jnp.pad(decay_jolt.reshape(2 * heads, rows), pad_rows)
    weights = (query_weight, key_weight, value_weight, glu_value_weight, glu_gate_weight)
    n_in = len(weights)
    dma = pltpu.SemaphoreType.DMA
    qkv, gated, pre = pl.pallas_call(
        functools.partial(project_kernel, n, nt, n_in),
        name="project",
        out_shape=(
            jax.ShapeDtypeStruct((rows, 3 * width), BF16),
            jax.ShapeDtypeStruct((rows, width), BF16),
            jax.ShapeDtypeStruct((rows, 128), F32),
        ),
        in_specs=[VM] * (3 + n_in),
        out_specs=(VM, VM, VM),
        scratch_shapes=[
            pltpu.VMEM((nt - 1, rows, part), BF16),
            pltpu.VMEM((n, rows, block), BF16),
            pltpu.VMEM((rows, n_in * width), F32),
            pltpu.VMEM((half - 1, n_in, block, width), BF16),
            pltpu.VMEM((half, n_in, block, width), BF16),
            dma((nt - 1,)), dma((nt - 1,)),
            dma((half - 1, n_in)), dma((half - 1, n_in)),
            dma((half, n_in)), dma((half, n_in)),
        ],
        compiler_params=pltpu.CompilerParams(collective_id=0, has_side_effects=True),
    )(inputs, in_gain.reshape(n, block), gate_weight, *weights)
    maps, reads, within = pl.pallas_call(
        functools.partial(delta_kernel, heads),
        name="delta",
        out_shape=(
            jax.ShapeDtypeStruct((2 * heads, HEAD, 2 * HEAD), BF16),
            jax.ShapeDtypeStruct((2 * heads, rows, HEAD), BF16),
            jax.ShapeDtypeStruct((heads, rows, HEAD), F32),
        ),
        in_specs=[VM] * 5,
        out_specs=(VM, VM, VM),
    )(qkv, pre, shift, pace, jolt)
    out_weight = jnp.concatenate([out_delta_weight, out_conv_weight], axis=0)
    out_rows, out_block = out_weight.shape
    out_width = out_block * n
    piece = rows // nt
    return pl.pallas_call(
        functools.partial(finish_kernel, n, nt, heads, channels),
        name="finish",
        out_shape=jax.ShapeDtypeStruct((piece, out_width), BF16),
        in_specs=[VM] * 8,
        out_specs=VM,
        scratch_shapes=[
            pltpu.VMEM((2, 2, heads, HEAD, 2 * HEAD), BF16),
            pltpu.VMEM((2, heads, HEAD, 2 * HEAD), BF16),
            pltpu.VMEM((2, half - 1, heads, HEAD, 2 * HEAD), BF16),
            pltpu.VMEM((2, 16, width), BF16),
            pltpu.VMEM((rows + 32, width), F32),
            pltpu.VMEM((8, rows), F32),
            pltpu.VMEM((nt - 1, 8, rows), F32),
            pltpu.VMEM((half - 1, out_rows, out_block), BF16),
            pltpu.VMEM((half, out_rows, out_block), BF16),
            pltpu.VMEM((nt, piece, out_width), BF16),
            pltpu.VMEM((nt - 1, piece, out_width), BF16),
            dma((2, 2)), dma((2, 2)),
            dma((2, half - 1)), dma((2, half - 1)),
            dma((2,)), dma((2,)),
            dma((nt - 1,)), dma((nt - 1,)),
            dma((half - 1,)), dma((half - 1,)),
            dma((half,)), dma((half,)),
            dma((nt - 1,)), dma((nt - 1,)),
        ],
        compiler_params=pltpu.CompilerParams(collective_id=1, has_side_effects=True),
    )(
        maps, reads, within, gated, conv_kernel, conv_gain.reshape(1, width),
        head_gain.reshape(1, HEAD), out_weight,
    )


def device_program(n, nt, *args):
    inputs, query_weight, pace = args[0], args[2], args[8]
    heads = pace.shape[1]
    block, width = query_weight.shape
    suits = (
        n % 2 == 0 and n >= 4 and nt >= 2
        and block % 128 == 0 and width % 128 == 0 and width == heads * HEAD
        and 2 * heads <= 8 and inputs.shape[1] % block == 0 and args[15].shape[1] % 128 == 0
        and args[13].shape[1] == width and V_HEADS == QK_HEADS
        and inputs.shape[0] & (inputs.shape[0] - 1) == 0
        and inputs.shape[0] % 128 == 0 and (inputs.shape[0] // nt) % 16 == 0
        and inputs.shape[0] <= 256 and KERNEL <= 33 and n <= 16
    )
    return fast_device(n, nt, *args) if suits else on_device(*args)


def solution(mesh):
    return jax.shard_map(
        functools.partial(device_program, mesh.shape["sp"], mesh.shape["tp"]),
        mesh=mesh,
        in_specs=(
            P("sp", "tp"),
            P(),
            P("sp", "tp"),
            P("sp", "tp"),
            P("sp", "tp"),
            P(),
            P(),
            P(),
            P(None, "tp", "sp"),
            P(None, "tp", "sp"),
            P(),
            P("sp", "tp"),
            P("sp", "tp"),
            P(None, "tp"),
            P("tp"),
            P("tp", "sp"),
            P("tp", "sp"),
        ),
        out_specs=P(("sp", "tp"), None),
        check_vma=False,
    )
```

profile of v0, /device:TPU:1, one launch (start us, length us, event | category | flops | bytes accessed | tf_op | source)
XLA Modules:
  0.0 163.3 jit_solution(2250651848129165517)
XLA Ops:
  0.0 0.0 copy-start
  0.0 0.9 dynamic-slice_bitcast_fusion
  1.0 0.3 copy.24
  1.3 0.0 copy-start.3
  1.3 0.9 pad.24.refs_2_
  2.2 0.0 copy-done.3
  2.2 0.6 reshape.24.refs_1_
  2.8 74.0 %project.1 = (bf16[256,768]{1,0:T(8,128)(2,1)}, bf16[256,256]{1,0:T(8,128)(2,1)}, f32[256,128]{1,0:T(8,128)}) custom-call(bf16[256,512]{1,0:T(8,128)(2,1)} %refs_0_.1, f32[8,256]{1,0:T(8,128)} %reshape.24.refs_1_, bf16[2048,128]{1,0:T(8,128)(2,1)} %pad.24.refs_2_, bf16[256,256]{1,0:T(8,128)(2,1)} %refs_3_.1, bf16[256,256]{1,0:T(8,128)(2,1)} %refs_4_.1, ...), custom_call_target="tpu_custom_call" | custom-call | tf_op jit(solution)/shard_map/project/pallas_call | solution.py:646
  76.8 0.0 copy-done
  76.8 0.1 constant_dynamic-slice_fusion
  76.9 0.1 reshape.32
  77.0 0.0 copy-start.4
  77.0 0.6 pad.25.shift_ref
  77.6 0.1 copy-done.4
  77.7 0.0 copy-start.5
  77.7 0.6 pad.26.pace_ref
  78.3 0.1 copy-done.5
  78.4 0.6 pad.27.jolt_ref
  79.0 22.1 %delta.1 = (bf16[4,128,256]{2,1,0:T(8,128)(2,1)}, bf16[4,256,128]{2,1,0:T(8,128)(2,1)}, f32[2,256,128]{2,1,0:T(8,128)}) custom-call(bf16[256,768]{1,0:T(8,128)(2,1)} %get-tuple-element.11.qkv_ref, f32[256,128]{1,0:T(8,128)} %get-tuple-element.12.pre_ref, f32[8,1]{1,0:T(8,128)} %pad.25.shift_ref, f32[8,256]{1,0:T(8,128)} %pad.26.pace_ref, f32[8,256]{1,0:T(8,128)} %pad.27.jolt_ref), custom_call_target="tpu_custom_call" | custom-call | tf_op jit(solution)/shard_map/delta/pallas_call | solution.py:668
  101.1 0.0 copy-done.1
  101.1 0.0 copy-done.2
  101.1 0.7 pad_maximum_fusion.ow_ref
  101.8 59.8 %finish.1 = bf16[64,2048]{1,0:T(8,128)(2,1)} custom-call(bf16[4,128,256]{2,1,0:T(8,128)(2,1)} %get-tuple-element.13.ma_ref, bf16[4,256,128]{2,1,0:T(8,128)(2,1)} %get-tuple-element.14.read_ref, f32[2,256,128]{2,1,0:T(8,128)} %get-tuple-element.15.within_ref, bf16[256,256]{1,0:T(8,128)(2,1)} %get-tuple-element.16.gated_ref, bf16[31,256]{1,0:T(8,128)(2,1)} %taps_ref.1, ...), custom_call_target="tpu_custom_call" | custom-call | tf_op jit(solution)/shard_map/finish/pallas_call | solution.py:683
  161.7 1.7 %copy.27 = bf16[64,2048]{1,0:T(8,128)(2,1)} copy(bf16[64,2048]{1,0:T(8,128)(2,1)} %finish.1) | data formatting | bytes 524288
  (7 shorter events, 0.1 us)
Async XLA Ops:
  0.0 76.8 %copy-start = (f32[2,8]{1,0:T(2,128)S(1)}, f32[2,8]{1,0:T(2,128)}, u32[]{:S(2)}) copy-start(f32[2,8]{1,0:T(2,128)} %param.24) | copy-start | bytes 196
  1.3 0.9 copy-start.3
  77.0 0.7 copy-start.4
  77.7 0.7 copy-start.5
  79.0 22.1 %copy-start.1 = (bf16[256,256]{1,0:T(8,128)(2,1)S(1)}, bf16[256,256]{1,0:T(8,128)(2,1)}, u32[]{:S(2)}) copy-start(bf16[256,256]{1,0:T(8,128)(2,1)} %param.33) | copy-start | bytes 393220
  79.0 22.1 %copy-start.2 = (bf16[256,256]{1,0:T(8,128)(2,1)S(1)}, bf16[256,256]{1,0:T(8,128)(2,1)}, u32[]{:S(2)}) copy-start(bf16[256,256]{1,0:T(8,128)(2,1)} %param.32) | copy-start | bytes 393220
where the time goes:
time: 164 us; the launch traced here: 163 us
  Pallas kernels  156 us (95%)
  local copies, waits for them, and re-layouts  6.59 us (4%)
    pallas_call x1, Pallas kernels, fast_device(): pl.pallas_call(functools.partial(project_kernel, n, nt, n_in), name='proj...  74 us
    pallas_call x1, Pallas kernels, fast_device(): pl.pallas_call(functools.partial(finish_kernel, n, nt, heads, channels),...  59.8 us
    pallas_call x1, Pallas kernels, fast_device(): pl.pallas_call(functools.partial(delta_kernel, heads), name='delta', out_...  22.1 us

commit v1 on v0

--- a/solution.py
+++ b/solution.py
@@ -312,113 +312,142 @@
     return jnp.dot(a, b, preferred_element_type=F32)
 
 
-def project_kernel(n, nt, n_in, *refs):
-    x_ref, gain_ref, wg_ref = refs[:3]
-    w_refs = refs[3 : 3 + n_in]
-    qkv_ref, gated_ref, pre_ref = refs[3 + n_in : 6 + n_in]
-    xbuf, normed, acc, wz, wx, xs, xr, zs, zr, ps, pr = refs[6 + n_in :]
+def dot3(a, b):
+    ah, bh = a.astype(BF16), b.astype(BF16)
+    al, bl = (a - ah.astype(F32)).astype(BF16), (b - bh.astype(F32)).astype(BF16)
+    return dot(ah, bh) + (dot(ah, bl) + dot(al, bh))
+
+
+def layer_kernel(n, nt, heads, channels, *refs):
+    (x_ref, gain_ref, wg_ref, shift_ref, pace_ref, jolt_ref, taps_ref, cgain_ref, hgain_ref) = refs[:9]
+    w_refs = refs[9:16]
+    out_ref = refs[16]
+    (
+        xbuf, normed, acc, wz, wx,
+        maps, reads, near, pair, far, halo, edges, conv_pad, stat, stats, part, parts,
+        xs, xr, zs, zr, ps, pr,
+        ns, nr, fs, fr, hs, hr, ss, sr, rs, rr,
+    ) = refs[17:]
     s, t, z, x, half, partner, stride = ring_peers(n)
     others = [(s, (t + d) % nt) for d in range(1, nt)]
-    greet(others + [partner] + stride)
-    order = [d for d in range(half - 1)]
+    greet(others + [((s + d) % n, t) for d in range(1, n)])
+    order = list(range(half - 1))
+    n_w = len(w_refs)
+    n_in = n_w - 2
+    rows, width_x = x_ref.shape
+    block, width = w_refs[0].shape
+
+    def came(d, side):
+        return ((z + half - 1 - d) % half) * 2 + side
+
     x_copies = [rcopy(x_ref, xbuf.at[d], xs.at[d], xr.at[d], others[d]) for d in range(nt - 1)]
     for c in x_copies:
         c.start()
-    own_x = [rcopy(w_refs[w], wx.at[0, w], ps.at[0, w], pr.at[0, w], partner) for w in range(n_in)]
+    own_x = [rcopy(w_refs[w], wx.at[0, w], ps.at[0, w], pr.at[0, w], partner) for w in range(n_w)]
     own_z = [
         [rcopy(w_refs[w], wz.at[d, w], zs.at[d, w], zr.at[d, w], stride[d]) for d in order]
-        for w in range(n_in)
+        for w in range(n_w)
     ]
-    for w in range(n_in):
+    forwards = [
+        [rcopy(wz.at[d, w], wx.at[d + 1, w], ps.at[d + 1, w], pr.at[d + 1, w], partner) for d in order]
+        for w in range(n_w)
+    ]
+
+    def send_z(w):
         for d in order:
             own_z[w][d].start()
+
+    for w in range(3):
+        send_z(w)
         own_x[w].start()
+    for w in range(3, n_w):
+        send_z(w)
     for c in x_copies:
         c.wait_recv()
-    rows, part = x_ref.shape
-    block = w_refs[0].shape[0]
-    per = part // block
-    total = rows * 0 + part * nt
+    per = width_x // block
+    depth = width_x * nt
     chunks = [(t, x_ref)] + [((t + nt - 1 - d) % nt, xbuf.at[d]) for d in range(nt - 1)]
-    mean = sum(jnp.sum(r[...].astype(F32), axis=1, keepdims=True) for _, r in chunks) / total
+    mean = sum(jnp.sum(r[...].astype(F32), axis=1, keepdims=True) for _, r in chunks) / depth
     var = (
         sum(jnp.sum(jnp.square(r[...].astype(F32) - mean), axis=1, keepdims=True) for _, r in chunks)
-        / total
+        / depth
     )
     inv = lax.rsqrt(var + 1e-05)
     for src, r in chunks:
         y = (r[...].astype(F32) - mean) * inv
         for p in range(per):
             b = src * per + p
-            g = gain_ref[pl.ds(b, 1), :]
+            g = gain_ref[:, pl.ds(pl.multiple_of(b * block, block), block)]
             normed[b] = (y[:, p * block : (p + 1) * block] * g).astype(BF16)
     pre = dot(normed[0], wg_ref[0:block, :])
     for b in range(1, n):
         pre = pre + dot(normed[b], wg_ref[b * block : (b + 1) * block, :])
-    pre_ref[...] = pre
-    width = w_refs[0].shape[1]
-    forwards = []
-    for w in range(n_in):
+
+    def relay(w):
+        for d in order:
+            own_z[w][d].wait_recv()
+            forwards[w][d].start()
+
+    def near_half(w):
         value = dot(normed[s], w_refs[w][...])
         for d in order:
-            own_z[w][d].wait_recv()
-            f = rcopy(wz.at[d, w], wx.at[d + 1, w], ps.at[d + 1, w], pr.at[d + 1, w], partner)
-            f.start()
-            forwards.append(f)
-            src = ((z + half - 1 - d) % half) * 2 + x
-            value = value + dot(normed[src], wz[d, w])
-        acc[:, w * width : (w + 1) * width] = value
-    for w in range(n_in):
+            value = value + dot(normed[came(d, x)], wz[d, w])
+        acc[w] = value
+
+    def far_half(w):
         own_x[w].wait_recv()
-        value = acc[:, w * width : (w + 1) * width]
-        value = value + dot(normed[z * 2 + (1 - x)], wx[0, w])
+        value = acc[w] + dot(normed[z * 2 + (1 - x)], wx[0, w])
         for d in order:
-            forwards[w * len(order) + d].wait_recv()
-            src = ((z + half - 1 - d) % half) * 2 + (1 - x)
-            value = value + dot(normed[src], wx[d + 1, w])
-        acc[:, w * width : (w + 1) * width] = value
-    qkv_ref[...] = acc[:, : 3 * width].astype(BF16)
-    glu_value = acc[:, 3 * width : 4 * width].astype(BF16).astype(F32)
-    glu_gate = acc[:, 4 * width : 5 * width].astype(BF16).astype(F32)
-    gated_ref[...] = (glu_value * jax.nn.sigmoid(glu_gate)).astype(BF16)
-    for c in x_copies + own_x + forwards + [c for row in own_z for c in row]:
-        c.wait_send()
-
-
-def dot3(a, b):
-    ah, bh = a.astype(BF16), b.astype(BF16)
-    al, bl = (a - ah.astype(F32)).astype(BF16), (b - bh.astype(F32)).astype(BF16)
-    return dot(ah, bh) + (dot(ah, bl) + dot(al, bh))
-
-
-def delta_kernel(heads, qkv_ref, pre_ref, shift_ref, pace_ref, jolt_ref, ma_ref, read_ref, within_ref):
-    span = qkv_ref.shape[0]
-    width = heads * HEAD
-    rows = jnp.transpose(pre_ref[...])
-    beta = jax.nn.sigmoid(rows[0:8] + shift_ref[...])
-    log_decay = -pace_ref[...] * jax.nn.softplus(rows[8:16]) + jolt_ref[...]
+            forwards[w][d].wait_recv()
+            value = value + dot(normed[came(d, 1 - x)], wx[d + 1, w])
+        acc[w] = value
+
+    for w in range(3):
+        relay(w)
+        near_half(w)
+    own_x[3].start()
+    own_x[4].start()
+    for w in range(3):
+        far_half(w)
+
+    span = rows
+    pre_rows = jnp.transpose(pre)
+    which = lax.broadcasted_iota(jnp.int32, (8, span), 0)
+    shift_lane = lax.broadcasted_iota(jnp.int32, shift_ref.shape, 1)
+    shift_rows = jnp.zeros((8, span), F32)
+    pace_rows = jnp.zeros((8, span), F32)
+    jolt_rows = jnp.zeros((8, span), F32)
+    for h in range(heads):
+        mine = jnp.sum(
+            jnp.where(shift_lane == t * heads + h, shift_ref[...], 0.0), axis=1, keepdims=True
+        )
+        for e in range(2):
+            here = which == e * heads + h
+            shift_rows = jnp.where(here, mine[e : e + 1, :], shift_rows)
+            pace_rows = jnp.where(here, pace_ref[e, h : h + 1, :], pace_rows)
+            jolt_rows = jnp.where(here, jolt_ref[e, h : h + 1, :], jolt_rows)
+    beta = jax.nn.sigmoid(pre_rows[0:8] + shift_rows)
+    log_decay = -pace_rows * jax.nn.softplus(pre_rows[8:16]) + jolt_rows
     i = lax.broadcasted_iota(jnp.int32, (span, span), 0)
     j = lax.broadcasted_iota(jnp.int32, (span, span), 1)
     high = lax.Precision.HIGHEST
     upto = jnp.dot(log_decay, (i <= j).astype(F32), precision=high, preferred_element_type=F32)
     onto = jnp.dot(log_decay, (i >= j).astype(F32), precision=high, preferred_element_type=F32)
-    which = lax.broadcasted_iota(jnp.int32, (8, span), 0)
     cum = jnp.where(which < heads, upto, onto)
-    cols = jnp.transpose(
-        jnp.concatenate([beta, cum, jnp.zeros((128 - 16, span), F32)], axis=0)
-    )
+    cols = jnp.transpose(jnp.concatenate([beta, cum, jnp.zeros((112, span), F32)], axis=0))
     eye = (i == j).astype(F32)
     eye_head = (
         lax.broadcasted_iota(jnp.int32, (HEAD, HEAD), 0)
         == lax.broadcasted_iota(jnp.int32, (HEAD, HEAD), 1)
     ).astype(F32)
     level = i ^ j
+    within = []
     for h in range(heads):
         lo = h * HEAD
-        q = jax.nn.silu(qkv_ref[:, lo : lo + HEAD].astype(F32))
-        k = jax.nn.silu(qkv_ref[:, width + lo : width + lo + HEAD].astype(F32))
+        q = jax.nn.silu(acc[0, :, lo : lo + HEAD].astype(BF16).astype(F32))
+        k = jax.nn.silu(acc[1, :, lo : lo + HEAD].astype(BF16).astype(F32))
         k = k * lax.rsqrt(jnp.sum(jnp.square(k), axis=1, keepdims=True) + 1e-06)
-        v = qkv_ref[:, 2 * width + lo : 2 * width + lo + HEAD].astype(F32)
+        v = acc[2, :, lo : lo + HEAD].astype(BF16).astype(F32)
         kt = jnp.transpose(k)
         kk = dot3(k, kt)
         qk = dot(q.astype(BF16), kt.astype(BF16))
@@ -444,26 +473,18 @@
             solved_b = solved.astype(BF16)
             out = dot((qk * decay).astype(BF16), solved_b)
             total = total + out[:, :HEAD]
-            read_ref[c] = (q * grown - out[:, HEAD:]).astype(BF16)
+            reads[c] = (q * grown - out[:, HEAD:]).astype(BF16)
             end = cum[c : c + 1, span - 1 : span] if e == 0 else cum[c : c + 1, 0:1]
             tail = jnp.transpose(k * jnp.exp(end - cum_col))
             state = dot3(tail, solved)
-            ma_ref[c, :, :HEAD] = (jnp.exp(end) * eye_head - state[:, HEAD:]).astype(BF16)
-            ma_ref[c, :, HEAD:] = state[:, :HEAD].astype(BF16)
-        within_ref[h] = total
-
-
-def finish_kernel(
-    n, nt, heads, channels,
-    ma_ref, read_ref, within_ref, gated_ref, taps_ref, cgain_ref, hgain_ref, ow_ref,
-    out_ref,
-    near, pair, far, halo, conv_pad, stat, stats, wz, wx, part, parts,
-    ns, nr, fs, fr, hs, hr, ss, sr, zs, zr, ps, pr, rs, rr,
-):
-    s, t, z, x, half, partner, stride = ring_peers(n)
-    others = [(s, (t + d) % nt) for d in range(1, nt)]
-    greet(others + [((s + d) % n, t) for d in range(1, n)])
-    rows, width = gated_ref.shape
+            maps[c, :, :HEAD] = (jnp.exp(end) * eye_head - state[:, HEAD:]).astype(BF16)
+            maps[c, :, HEAD:] = state[:, :HEAD].astype(BF16)
+        within.append(total)
+        if h < 2:
+            relay(3 + h)
+    for w in range(3 + min(heads, 2), n_in):
+        relay(w)
+
     edge = 16
 
     def at(offset):
@@ -471,17 +492,6 @@
 
     def inside(offset):
         return (s < n - offset) if offset > 0 else (s >= -offset)
-
-    steps = []
-    for d in (1, 2):
-        for e in range(2):
-            go = d if e == 0 else -d
-            lo = e * heads
-            steps.append((go, rcopy(ma_ref.at[pl.ds(lo, heads)], near.at[e, d - 1], ns.at[e, d - 1], nr.at[e, d - 1], at(go)), near.at[e, d - 1]))
-    sides = [
-        (1, rcopy(gated_ref.at[pl.ds(rows - edge, edge)], halo.at[0], hs.at[0], hr.at[0], at(1)), halo.at[0]),
-        (-1, rcopy(gated_ref.at[pl.ds(0, edge)], halo.at[1], hs.at[1], hr.at[1], at(-1)), halo.at[1]),
-    ]
 
     def start(moves):
         for go, copy, _ in moves:
@@ -505,13 +515,28 @@
             def _():
                 copy.wait_send()
 
+    steps = []
+    for d in (1, 2):
+        for e in range(2):
+            go = d if e == 0 else -d
+            slot = near.at[e, d - 1]
+            steps.append((go, rcopy(maps.at[pl.ds(e * heads, heads)], slot, ns.at[e, d - 1], nr.at[e, d - 1], at(go)), slot))
     start(steps)
+
+    for w in range(3, n_in):
+        near_half(w)
+    for w in range(3, n_in):
+        far_half(w)
+    glu_value = acc[3].astype(BF16).astype(F32)
+    glu_gate = acc[4].astype(BF16).astype(F32)
+    gated = (glu_value * jax.nn.sigmoid(glu_gate)).astype(BF16)
+    edges[0] = gated[0:edge]
+    edges[1] = gated[rows - edge : rows]
+    sides = [
+        (1, rcopy(edges.at[1], halo.at[0], hs.at[0], hr.at[0], at(1)), halo.at[0]),
+        (-1, rcopy(edges.at[0], halo.at[1], hs.at[1], hr.at[1], at(-1)), halo.at[1]),
+    ]
     start(sides)
-    own_z = [rcopy(ow_ref, wz.at[d], zs.at[d], zr.at[d], stride[d]) for d in range(half - 1)]
-    own_x = rcopy(ow_ref, wx.at[0], ps.at[0], pr.at[0], partner)
-    own_x.start()
-    for c in own_z:
-        c.start()
     arrive(steps)
     for e in range(2):
         for h in range(heads):
@@ -523,12 +548,16 @@
     for d in range(1, half):
         for e in range(2):
             go = 2 * d if e == 0 else -2 * d
-            hops.append((go, rcopy(pair.at[e], far.at[e, d - 1], fs.at[e, d - 1], fr.at[e, d - 1], at(go)), far.at[e, d - 1]))
+            slot = far.at[e, d - 1]
+            hops.append((go, rcopy(pair.at[e], slot, fs.at[e, d - 1], fr.at[e, d - 1], at(go)), slot))
     start(hops)
-
+    for w in range(n_in, n_w):
+        own_x[w].start()
+    relay(n_in)
+
+    conv_pad[edge : edge + rows, :] = gated.astype(F32)
     arrive(sides)
     conv_pad[0:edge, :] = halo[0].astype(F32)
-    conv_pad[edge : edge + rows, :] = gated_ref[...].astype(F32)
     conv_pad[edge + rows : 2 * edge + rows, :] = halo[1].astype(F32)
     taps = taps_ref[...].astype(F32)
     count = taps.shape[0]
@@ -543,14 +572,8 @@
     stat_copies = [rcopy(stat, stats.at[d], ss.at[d], sr.at[d], others[d]) for d in range(nt - 1)]
     for c in stat_copies:
         c.start()
-
-    forwards = []
-    for d in range(half - 1):
-        own_z[d].wait_recv()
-        f = rcopy(wz.at[d], wx.at[d + 1], ps.at[d + 1], pr.at[d + 1], partner)
-        f.start()
-        forwards.append(f)
-
+    for w in range(n_in + 1, n_w):
+        relay(w)
     for c in stat_copies:
         c.wait_recv()
     whole = stat[...]
@@ -566,7 +589,7 @@
     arrive(hops)
     delta_heads = []
     for h in range(heads):
-        o = within_ref[h]
+        o = within[h]
         for e in range(2):
             entry = jnp.zeros((HEAD, HEAD), F32)
             for d in range(half - 2, -1, -1):
@@ -574,41 +597,53 @@
                 entry = dot(m[:, :HEAD], entry.astype(BF16)) + m[:, HEAD:].astype(F32)
             m = pair[e, h]
             entry = dot(m[:, :HEAD], entry.astype(BF16)) + m[:, HEAD:].astype(F32)
-            o = o + dot(read_ref[e * heads + h], entry.astype(BF16))
+            o = o + dot(reads[e * heads + h], entry.astype(BF16))
         o = o * lax.rsqrt(jnp.mean(jnp.square(o), axis=1, keepdims=True) + 1e-06) * hgain_ref[...]
         delta_heads.append(o.astype(BF16))
-    both = jnp.concatenate(delta_heads + [conv_out], axis=1)
-    block = ow_ref.shape[1]
+    delta_out = jnp.concatenate(delta_heads, axis=1)
     piece = rows // nt
-
-    def emit(src, weights):
-        value = dot(both, weights).astype(BF16)
-        column = pl.ds(pl.multiple_of(src * block, block), block)
+    sums = []
+
+    def emit(first, second):
+        at_block = len(sums)
+        value = (dot(delta_out, first) + dot(conv_out, second)).astype(BF16)
         for p in range(nt):
-            part[p, :, column] = value[p * piece : (p + 1) * piece]
-
-    emit(s, ow_ref[...])
-    for d in range(half - 1):
-        emit(((z + half - 1 - d) % half) * 2 + x, wz[d])
-    own_x.wait_recv()
-    emit(z * 2 + (1 - x), wx[0])
-    for d in range(half - 1):
-        forwards[d].wait_recv()
-        emit(((z + half - 1 - d) % half) * 2 + (1 - x), wx[d + 1])
-    sums = [rcopy(part.at[(t + d) % nt], parts.at[d - 1], rs.at[d - 1], rr.at[d - 1], others[d - 1]) for d in range(1, nt)]
-    for c in sums:
-        c.start()
-    for c in sums:
-        c.wait_recv()
-    mixed = part[t].astype(F32)
-    for d in range(nt - 1):
-        mixed = mixed + parts[d].astype(F32)
-    out_ref[...] = mixed.astype(BF16)
+            part[at_block, p] = value[p * piece : (p + 1) * piece]
+        copies = [
+            rcopy(part.at[at_block, (t + d) % nt], parts.at[d - 1, at_block], rs.at[d - 1, at_block], rr.at[d - 1, at_block], others[d - 1])
+            for d in range(1, nt)
+        ]
+        for c in copies:
+            c.start()
+        sums.append(copies)
+
+    sources = [s]
+    emit(w_refs[n_in][...], w_refs[n_in + 1][...])
+    for d in order:
+        sources.append(came(d, x))
+        emit(wz[d, n_in], wz[d, n_in + 1])
+    sources.append(z * 2 + (1 - x))
+    own_x[n_in].wait_recv()
+    own_x[n_in + 1].wait_recv()
+    emit(wx[0, n_in], wx[0, n_in + 1])
+    for d in order:
+        forwards[n_in][d].wait_recv()
+        forwards[n_in + 1][d].wait_recv()
+        sources.append(came(d, 1 - x))
+        emit(wx[d + 1, n_in], wx[d + 1, n_in + 1])
+    out_block = w_refs[n_in].shape[1]
+    for b in range(n):
+        mixed = part[b, t].astype(F32)
+        for d in range(nt - 1):
+            sums[b][d].wait_recv()
+            mixed = mixed + parts[d, b].astype(F32)
+        out_ref[:, pl.ds(pl.multiple_of(sources[b] * out_block, out_block), out_block)] = mixed.astype(BF16)
     left(steps)
     left(sides)
     left(hops)
-    for c in own_z + [own_x] + forwards + stat_copies + sums:
-        c.wait_send()
+    for group in own_z + forwards + sums + [x_copies, own_x, stat_copies]:
+        for c in group:
+            c.wait_send()
 
 
 def fast_device(
@@ -617,7 +652,7 @@
     beta_shift, decay_pace, decay_jolt, head_gain, glu_value_weight, glu_gate_weight,
     conv_kernel, conv_gain, out_delta_weight, out_conv_weight,
 ):
-    rows, part = inputs.shape
+    rows, width_x = inputs.shape
     block, width = query_weight.shape
     heads = decay_pace.shape[1]
     half = n // 2
@@ -634,82 +669,51 @@
         jnp.concatenate([gate_columns(beta_weight), gate_columns(decay_weight)], axis=1),
         ((0, 0), (0, 112)),
     )
-    pad_rows = ((0, 8 - 2 * heads), (0, 0))
-    shift = jnp.pad(
-        lax.dynamic_slice_in_dim(beta_shift, first, heads, 1).reshape(2 * heads, 1), pad_rows
-    )
-    pace = jnp.pad(decay_pace.reshape(2 * heads, rows), pad_rows)
-    jolt = jnp.pad(decay_jolt.reshape(2 * heads, rows), pad_rows)
-    weights = (query_weight, key_weight, value_weight, glu_value_weight, glu_gate_weight)
-    n_in = len(weights)
+    weights = (
+        query_weight, key_weight, value_weight, glu_value_weight, glu_gate_weight,
+        out_delta_weight, out_conv_weight,
+    )
+    n_w = len(weights)
+    out_block = out_delta_weight.shape[1]
+    piece = rows // nt
     dma = pltpu.SemaphoreType.DMA
-    qkv, gated, pre = pl.pallas_call(
-        functools.partial(project_kernel, n, nt, n_in),
-        name="project",
-        out_shape=(
-            jax.ShapeDtypeStruct((rows, 3 * width), BF16),
-            jax.ShapeDtypeStruct((rows, width), BF16),
-            jax.ShapeDtypeStruct((rows, 128), F32),
-        ),
-        in_specs=[VM] * (3 + n_in),
-        out_specs=(VM, VM, VM),
-        scratch_shapes=[
-            pltpu.VMEM((nt - 1, rows, part), BF16),
-            pltpu.VMEM((n, rows, block), BF16),
-            pltpu.VMEM((rows, n_in * width), F32),
-            pltpu.VMEM((half - 1, n_in, block, width), BF16),
-            pltpu.VMEM((half, n_in, block, width), BF16),
-            dma((nt - 1,)), dma((nt - 1,)),
-            dma((half - 1, n_in)), dma((half - 1, n_in)),
-            dma((half, n_in)), dma((half, n_in)),
-        ],
-        compiler_params=pltpu.CompilerParams(collective_id=0, has_side_effects=True),
-    )(inputs, in_gain.reshape(n, block), gate_weight, *weights)
-    maps, reads, within = pl.pallas_call(
-        functools.partial(delta_kernel, heads),
-        name="delta",
-        out_shape=(
-            jax.ShapeDtypeStruct((2 * heads, HEAD, 2 * HEAD), BF16),
-            jax.ShapeDtypeStruct((2 * heads, rows, HEAD), BF16),
-            jax.ShapeDtypeStruct((heads, rows, HEAD), F32),
-        ),
-        in_specs=[VM] * 5,
-        out_specs=(VM, VM, VM),
-    )(qkv, pre, shift, pace, jolt)
-    out_weight = jnp.concatenate([out_delta_weight, out_conv_weight], axis=0)
-    out_rows, out_block = out_weight.shape
-    out_width = out_block * n
-    piece = rows // nt
     return pl.pallas_call(
-        functools.partial(finish_kernel, n, nt, heads, channels),
-        name="finish",
-        out_shape=jax.ShapeDtypeStruct((piece, out_width), BF16),
-        in_specs=[VM] * 8,
+        functools.partial(layer_kernel, n, nt, heads, channels),
+        name="layer",
+        out_shape=jax.ShapeDtypeStruct((piece, out_block * n), BF16),
+        in_specs=[VM] * (9 + n_w),
         out_specs=VM,
         scratch_shapes=[
+            pltpu.VMEM((nt - 1, rows, width_x), BF16),
+            pltpu.VMEM((n, rows, block), BF16),
+            pltpu.VMEM((n_w - 2, rows, width), F32),
+            pltpu.VMEM((half - 1, n_w, block, width), BF16),
+            pltpu.VMEM((half, n_w, block, width), BF16),
+            pltpu.VMEM((2 * heads, HEAD, 2 * HEAD), BF16),
+            pltpu.VMEM((2 * heads, rows, HEAD), BF16),
             pltpu.VMEM((2, 2, heads, HEAD, 2 * HEAD), BF16),
             pltpu.VMEM((2, heads, HEAD, 2 * HEAD), BF16),
             pltpu.VMEM((2, half - 1, heads, HEAD, 2 * HEAD), BF16),
             pltpu.VMEM((2, 16, width), BF16),
+            pltpu.VMEM((2, 16, width), BF16),
             pltpu.VMEM((rows + 32, width), F32),
             pltpu.VMEM((8, rows), F32),
             pltpu.VMEM((nt - 1, 8, rows), F32),
-            pltpu.VMEM((half - 1, out_rows, out_block), BF16),
-            pltpu.VMEM((half, out_rows, out_block), BF16),
-            pltpu.VMEM((nt, piece, out_width), BF16),
-            pltpu.VMEM((nt - 1, piece, out_width), BF16),
+            pltpu.VMEM((n, nt, piece, out_block), BF16),
+            pltpu.VMEM((nt - 1, n, piece, out_block), BF16),
+            dma((nt - 1,)), dma((nt - 1,)),
+            dma((half - 1, n_w)), dma((half - 1, n_w)),
+            dma((half, n_w)), dma((half, n_w)),
             dma((2, 2)), dma((2, 2)),
             dma((2, half - 1)), dma((2, half - 1)),
             dma((2,)), dma((2,)),
             dma((nt - 1,)), dma((nt - 1,)),
-            dma((half - 1,)), dma((half - 1,)),
-            dma((half,)), dma((half,)),
-            dma((nt - 1,)), dma((nt - 1,)),
+            dma((nt - 1, n)), dma((nt - 1, n)),
         ],
-        compiler_params=pltpu.CompilerParams(collective_id=1, has_side_effects=True),
+        compiler_params=pltpu.CompilerParams(collective_id=0, has_side_effects=True),
     )(
-        maps, reads, within, gated, conv_kernel, conv_gain.reshape(1, width),
-        head_gain.reshape(1, HEAD), out_weight,
+        inputs, in_gain.reshape(1, depth), gate_weight, beta_shift, decay_pace, decay_jolt,
+        conv_kernel, conv_gain.reshape(1, width), head_gain.reshape(1, HEAD), *weights,
     )
 
 
@@ -721,7 +725,7 @@
         n % 2 == 0 and n >= 4 and nt >= 2
         and block % 128 == 0 and width % 128 == 0 and width == heads * HEAD
         and 2 * heads <= 8 and inputs.shape[1] % block == 0 and args[15].shape[1] % 128 == 0
-        and args[13].shape[1] == width and V_HEADS == QK_HEADS
+        and args[13].shape[1] == width and args[15].shape == (block, width) and V_HEADS == QK_HEADS
         and inputs.shape[0] & (inputs.shape[0] - 1) == 0
         and inputs.shape[0] % 128 == 0 and (inputs.shape[0] // nt) % 16 == 0
         and inputs.shape[0] <= 256 and KERNEL <= 33 and n <= 16

time: 164 us -> 130 us (0.79)
  the two profiles are of different devices: /device:TPU:1 before, /device:TPU:11 now
where the time goes in v1:
time: 130 us
  Pallas kernels  126 us (97%)
  local copies, waits for them, and re-layouts  3.77 us (3%)
    pallas_call x1, Pallas kernels, fast_device(): pl.pallas_call(functools.partial(layer_kernel, n, nt, heads, channels), n...  126 us

profile of v1, /device:TPU:11, one launch (start us, length us, event | category | flops | bytes accessed | tf_op | source)
XLA Modules:
  0.0 129.8 jit_solution(4689245898671351875)
XLA Ops:
  0.0 0.9 dynamic-slice_bitcast_fusion
  1.0 0.3 copy.22
  1.3 0.9 pad.13.refs_2_
  2.1 126.0 %layer.1 = bf16[64,2048]{1,0:T(8,128)(2,1)} custom-call(bf16[256,512]{1,0:T(8,128)(2,1)} %refs_0_.1, f32[1,2048]{1,0:T(1,128)} %bitcast.11, bf16[2048,128]{1,0:T(8,128)(2,1)} %pad.13.refs_2_, f32[2,8]{1,0:T(2,128)} %refs_3_.1, f32[2,2,256]{2,1,0:T(2,128)} %refs_4_.1, f32[2,2,256]{2,1,0:T(2,128)} %refs_5_.1, bf16[31,256]{1,0:T(8,128)(2,1)} %refs_6_.1, ...), custom_call_target="tpu_custom_call" | custom-call | tf_op jit(solution)/shard_map/layer/pallas_call | solution.py:680
  128.2 1.7 %copy.24 = bf16[64,2048]{1,0:T(8,128)(2,1)} copy(bf16[64,2048]{1,0:T(8,128)(2,1)} %layer.1) | data formatting | bytes 524288
  (3 shorter events, 0.0 us)

commit v2 on v1

--- a/solution.py
+++ b/solution.py
@@ -465,8 +465,12 @@
             size = 2
             while size < span:
                 corner = jnp.where((level >= size) & (level < 2 * size), below, 0.0)
-                inverse = inverse - dot3(inverse, dot3(corner, inverse))
+                low = inverse.astype(BF16)
+                reach = dot(corner.astype(BF16), low)
+                inverse = inverse - dot(low, reach.astype(BF16))
                 size = 2 * size
+            residual = (eye - inverse) - dot3(below, inverse)
+            inverse = inverse + dot(inverse.astype(BF16), residual.astype(BF16))
             grown = jnp.exp(cum_col)
             rhs = jnp.concatenate([v * beta_col, k * (beta_col * grown)], axis=1)
             solved = dot3(inverse, rhs)
@@ -479,11 +483,9 @@
             state = dot3(tail, solved)
             maps[c, :, :HEAD] = (jnp.exp(end) * eye_head - state[:, HEAD:]).astype(BF16)
             maps[c, :, HEAD:] = state[:, :HEAD].astype(BF16)
+            if h == 0:
+                relay(3 + e)
         within.append(total)
-        if h < 2:
-            relay(3 + h)
-    for w in range(3 + min(heads, 2), n_in):
-        relay(w)
 
     edge = 16
 
@@ -522,6 +524,8 @@
             slot = near.at[e, d - 1]
             steps.append((go, rcopy(maps.at[pl.ds(e * heads, heads)], slot, ns.at[e, d - 1], nr.at[e, d - 1], at(go)), slot))
     start(steps)
+    own_x[n_in].start()
+    relay(n_in)
 
     for w in range(3, n_in):
         near_half(w)
@@ -551,9 +555,8 @@
             slot = far.at[e, d - 1]
             hops.append((go, rcopy(pair.at[e], slot, fs.at[e, d - 1], fr.at[e, d - 1], at(go)), slot))
     start(hops)
-    for w in range(n_in, n_w):
+    for w in range(n_in + 1, n_w):
         own_x[w].start()
-    relay(n_in)
 
     conv_pad[edge : edge + rows, :] = gated.astype(F32)
     arrive(sides)

time: 130 us -> 129 us (level)
  Pallas kernels: 126 us -> 124 us
    pallas_call x1, Pallas kernels: 126 us -> 124 us  [fast_device(): pl.pallas_call(functools.partial(layer_kernel, n, nt, heads, channels), n...]
where the time goes in v2:
time: 129 us; the launch traced here: 128 us
  Pallas kernels  124 us (96%)
  local copies, waits for them, and re-layouts  3.77 us (3%)
    pallas_call x1, Pallas kernels, fast_device(): pl.pallas_call(functools.partial(layer_kernel, n, nt, heads, channels), n...  124 us

profile of v2, /device:TPU:11, one launch (start us, length us, event | category | flops | bytes accessed | tf_op | source)
XLA Modules:
  0.0 128.3 jit_solution(2905420694924936255)
XLA Ops:
  0.0 0.9 dynamic-slice_bitcast_fusion
  1.0 0.3 copy.22
  1.3 0.9 pad.13.refs_2_
  2.1 124.5 %layer.1 = bf16[64,2048]{1,0:T(8,128)(2,1)} custom-call(bf16[256,512]{1,0:T(8,128)(2,1)} %refs_0_.1, f32[1,2048]{1,0:T(1,128)} %bitcast.11, bf16[2048,128]{1,0:T(8,128)(2,1)} %pad.13.refs_2_, f32[2,8]{1,0:T(2,128)} %refs_3_.1, f32[2,2,256]{2,1,0:T(2,128)} %refs_4_.1, f32[2,2,256]{2,1,0:T(2,128)} %refs_5_.1, bf16[31,256]{1,0:T(8,128)(2,1)} %refs_6_.1, ...), custom_call_target="tpu_custom_call" | custom-call | tf_op jit(solution)/shard_map/layer/pallas_call | solution.py:683
  126.6 1.7 %copy.24 = bf16[64,2048]{1,0:T(8,128)(2,1)} copy(bf16[64,2048]{1,0:T(8,128)(2,1)} %layer.1) | data formatting | bytes 524288
  (3 shorter events, 0.0 us)
